TPU v7x, 512 devices: a whole 4x8x8 slice. The times are simulated.
512 devices in a mesh: sp: 32 (over z, x), tp: 16 (over y, core).
Axes of the slice: x: 4, y: 8, z: 8, core: 2. Of those that a mesh axis runs over, the one named last changes fastest.
Arguments:
- stream_in: bfloat16 [4096, 2048], P('sp'), may hold values from -8 to 8
- out_cot: bfloat16 [4096, 2048], P('sp'), may hold values from -6 to 6
- route_experts: int32 [4096, 2], P('sp'), may hold values from 0 to 31, all different within a row; in each aligned block of 128 rows (0 to 127, 128 to 255, ...) at most 16 rows name the same one
- route_weights: float32 [4096, 2], P('sp'), may hold values from 0.1 to 1
- w_gate: bfloat16 [32, 2048, 2048], P('sp', None, 'tp'), may hold values from -0.125 to 0.125
- w_up: bfloat16 [32, 2048, 2048], P('sp', None, 'tp'), may hold values from -0.125 to 0.125
- w_down: bfloat16 [32, 2048, 2048], P('sp', 'tp'), may hold values from -0.125 to 0.125
- w_proj: bfloat16 [2048, 1024], P(None, 'tp'), may hold values from -0.1875 to 0.1875
- conv_value: bfloat16 [1024, 4096], P('tp', 'sp'), may hold values from -6 to 6
- conv_gate: bfloat16 [1024, 4096], P('tp', 'sp'), may hold values from -8 to 8
- conv_taps: float32 [31, 1024], P(None, 'tp'), may hold values from -1 to 1
- conv_result: bfloat16 [1024, 4096], P('tp', 'sp'), may hold values from -100 to 100
- channel_norm_gain: float32 [1024], P('tp'), may hold values from 0.1 to 1.9
Outputs:
- grad_gate: bfloat16 [32, 2048, 2048], P('sp', None, 'tp')
- grad_up: bfloat16 [32, 2048, 2048], P('sp', None, 'tp')
- grad_down: bfloat16 [32, 2048, 2048], P('sp', 'tp')
- grad_stream: bfloat16 [4096, 2048], P('sp')
- grad_proj: float32 [2048, 1024], P('sp', 'tp')
- grad_value: bfloat16 [1024, 4096], P('tp', 'sp')
- grad_gate_in: bfloat16 [1024, 4096], P('tp', 'sp')
Inputs may be any that keep to these rules, and one draw needn't show every extreme that they name: `route_experts`: each row names 2 different experts; within each aligned block of 128 rows no expert is named by more than 16 rows, and at least one block reaches that bound for some expert.
All inputs are finite; a program needn't handle non-finite values.
Results may differ from a plain program's by a relative error of at most 0.025.
Values may be sent and summed in bfloat16 or wider, within the bound.
No kernel may reach another device: no remote copies, remote signals or barrier semaphores. Data moves between devices by JAX's collectives and lax.ppermute only.
A program may use at most 64 MiB of HBM per device.

v0:
```python
import jax
import jax.numpy as jnp
from jax import lax
from jax.sharding import PartitionSpec as P

norm_eps = 1e-05
clamp_limit = 7.0
alpha_gate = 1.702


def sent_together(arrays, axis, split_dim, concat_dim, along):
    widths = [a.shape[along] for a in arrays]
    both = jnp.concatenate(arrays, axis=along)
    filled = lax.all_to_all(both, axis, split_axis=split_dim, concat_axis=concat_dim, tiled=True)
    return tuple(jnp.split(filled, [sum(widths[:k]) for k in range(1, len(widths))], axis=along))


def sent_together_2(arrays, axis, dim, along):
    ends, at = ([], 0)
    for a in arrays[:-1]:
        at += a.shape[along]
        ends.append(at)
    both = jnp.concatenate(arrays, axis=along)
    return tuple(jnp.split(lax.all_gather(both, axis, axis=dim, tiled=True), ends, axis=along))


def cut_along(array, dim, devices):
    before, after = (array.shape[:dim], array.shape[dim + 1 :])
    return jnp.moveaxis(array.reshape(*before, devices, -1, *after), dim, 0)


def summed_on_arrival(array, axis, dim):
    tiles = cut_along(array, dim, lax.axis_size(axis))
    arrived = lax.all_to_all(tiles, axis, split_axis=0, concat_axis=0, tiled=True)
    return arrived.astype(jnp.float32).sum(axis=0)


def copy_for_each(array, axis):
    copies = jnp.broadcast_to(array, (lax.axis_size(axis), *array.shape))
    return lax.all_to_all(copies, axis, split_axis=0, concat_axis=0, tiled=True)


def taken_together(array, axis):
    return copy_for_each(array, axis).sum(axis=0)


def packed_total(arrays, axis):
    ends = [0]
    for a in arrays:
        ends.append(ends[-1] + a.size)
    so_far = taken_together(jnp.concatenate([a.ravel() for a in arrays]), axis)
    return tuple((so_far[b:e].reshape(a.shape) for a, b, e in zip(arrays, ends, ends[1:])))


def summed_on_arrival_2(array, axis, dim):
    devices = lax.axis_size(axis)
    tiles = lax.all_to_all(cut_along(array, dim, devices), axis, 0, 0, tiled=True)
    return jnp.sum(tiles, axis=0)


def from_behind(value, axis, steps):
    count = lax.axis_size(axis)
    leading, last = (max(0, -steps), min(count, count - steps))
    return lax.ppermute(value, axis, [(source, source + steps) for source in range(leading, last)])


def slot_tables(block_routes, experts_all, capacity):
    flat_routes = block_routes.reshape(-1)
    assigns = flat_routes.shape[0]
    onehot = (flat_routes[:, None] == jnp.arange(experts_all, dtype=jnp.int32)[None, :]).astype(
        jnp.int32
    )
    before = jnp.cumsum(onehot, axis=0) - onehot
    rank_in = jnp.sum(before * onehot, axis=1)
    slot_of = flat_routes * capacity + rank_in
    source_of = (
        jnp.full((experts_all * capacity,), -1, jnp.int32)
        .at[slot_of]
        .set(jnp.arange(assigns, dtype=jnp.int32))
    )
    return (slot_of, source_of)


def combine_routes(returned, slot_of, cot_cols, token_rows, top_count):
    feature_count = returned.shape[-1]
    flat_back = returned.reshape(-1, feature_count)
    per_route = flat_back[slot_of].astype(jnp.float32).reshape(token_rows, top_count, feature_count)
    return (cot_cols.astype(jnp.float32) + jnp.sum(per_route, axis=1)).astype(jnp.bfloat16)


def expert_terms(rows_in, cot_in, w_gate, w_up, w_down):
    pre_gate = jnp.einsum("secd,edf->secf", rows_in, w_gate, preferred_element_type=jnp.float32)
    pre_up = jnp.einsum("secd,edf->secf", rows_in, w_up, preferred_element_type=jnp.float32)
    glu_part = jnp.minimum(pre_gate, clamp_limit)
    lin_part = jnp.clip(pre_up, -clamp_limit, clamp_limit)
    sig_glu = jax.nn.sigmoid(alpha_gate * glu_part)
    activated = (glu_part * sig_glu * (lin_part + 1.0)).astype(jnp.bfloat16)
    grad_act = jnp.einsum("secd,efd->secf", cot_in, w_down, preferred_element_type=jnp.float32)
    slope = sig_glu + alpha_gate * glu_part * sig_glu * (1.0 - sig_glu)
    grad_pre_gate = jnp.where(
        pre_gate < clamp_limit, grad_act * (lin_part + 1.0) * slope, 0.0
    ).astype(jnp.bfloat16)
    grad_pre_up = jnp.where(
        jnp.abs(pre_up) < clamp_limit, grad_act * glu_part * sig_glu, 0.0
    ).astype(jnp.bfloat16)
    grad_down = jnp.einsum(
        "secf,secd->efd", activated, cot_in, preferred_element_type=jnp.float32
    ).astype(jnp.bfloat16)
    grad_gate = jnp.einsum(
        "secd,secf->edf", rows_in, grad_pre_gate, preferred_element_type=jnp.float32
    ).astype(jnp.bfloat16)
    grad_up = jnp.einsum(
        "secd,secf->edf", rows_in, grad_pre_up, preferred_element_type=jnp.float32
    ).astype(jnp.bfloat16)
    input_part = jnp.einsum(
        "secf,edf->secd", grad_pre_gate, w_gate, preferred_element_type=jnp.float32
    )
    input_part = input_part + jnp.einsum(
        "secf,edf->secd", grad_pre_up, w_up, preferred_element_type=jnp.float32
    )
    return (grad_gate, grad_up, grad_down, input_part)


def body(
    stream_in,
    out_cot,
    route_experts,
    route_weights,
    w_gate,
    w_up,
    w_down,
    w_proj,
    conv_value,
    conv_gate,
    conv_taps,
    conv_result,
    channel_norm_gain,
):
    sp_count = lax.axis_size("sp")
    tp_count = lax.axis_size("tp")
    local_experts = w_gate.shape[0]
    experts_all = local_experts * sp_count
    token_rows, model_width = stream_in.shape
    top_count = route_experts.shape[1]
    capacity = 2 * top_count * token_rows // experts_all
    slot_of, source_of = slot_tables(route_experts, experts_all, capacity)
    occupied = source_of >= 0
    source_safe = jnp.maximum(source_of, 0)
    token_of = source_safe // top_count
    slot_weight = jnp.where(occupied, route_weights.reshape(-1)[source_safe], 0.0)
    row_buffer = jnp.where(occupied[:, None], stream_in[token_of], jnp.zeros((), jnp.bfloat16))
    cot_buffer = (slot_weight[:, None] * out_cot[token_of].astype(jnp.float32)).astype(jnp.bfloat16)
    row_buffer = row_buffer.reshape(experts_all, capacity, model_width)
    cot_buffer = cot_buffer.reshape(experts_all, capacity, model_width)
    slice_width = model_width // tp_count
    slice_start = lax.axis_index("tp") * slice_width
    row_slice = lax.dynamic_slice_in_dim(row_buffer, slice_start, slice_width, 2)
    cot_slice = lax.dynamic_slice_in_dim(cot_buffer, slice_start, slice_width, 2)
    row_slice, cot_slice = sent_together((row_slice, cot_slice), "sp", 0, 0, 1)
    rows_in, cot_in = sent_together_2((row_slice, cot_slice), "tp", 2, 0)
    rows_in = rows_in.reshape(sp_count, local_experts, capacity, model_width)
    cot_in = cot_in.reshape(sp_count, local_experts, capacity, model_width)
    grad_gate, grad_up, grad_down, input_part = expert_terms(rows_in, cot_in, w_gate, w_up, w_down)
    shared = summed_on_arrival(input_part.astype(jnp.bfloat16), "tp", 3)
    returned = shared.astype(jnp.bfloat16).reshape(experts_all, capacity, slice_width)
    returned = lax.all_to_all(returned, "sp", split_axis=0, concat_axis=0, tiled=True)
    cot_cols = lax.dynamic_slice_in_dim(out_cot, slice_start, slice_width, 1)
    stream_part = combine_routes(returned, slot_of, cot_cols, token_rows, top_count)
    grad_stream = lax.all_gather(stream_part, "tp", axis=1, tiled=True)
    channel_total = conv_result.shape[0] * tp_count
    positions = conv_result.shape[1]
    conv_float = conv_result.astype(jnp.float32)
    chan_sum, chan_sq = packed_total(
        (jnp.sum(conv_float, axis=0), jnp.sum(conv_float * conv_float, axis=0)), "tp"
    )
    chan_mean = chan_sum / channel_total
    chan_var = chan_sq / channel_total - chan_mean * chan_mean
    inverse_deviation = lax.rsqrt(chan_var + norm_eps)
    mean_removed = (conv_float - chan_mean) * inverse_deviation
    normalized_rows = mean_removed * channel_norm_gain[:, None]
    sigmoid_of_norm = jax.nn.sigmoid(normalized_rows)
    hidden = (normalized_rows * sigmoid_of_norm).astype(jnp.bfloat16)
    grad_proj = summed_on_arrival_2(
        lax.dot_general(
            grad_stream, hidden, (((0,), (1,)), ((), ())), preferred_element_type=jnp.float32
        ),
        "sp",
        0,
    )
    hidden_gradient = lax.dot_general(
        w_proj, grad_stream, (((0,), (1,)), ((), ())), preferred_element_type=jnp.float32
    )
    normed_input_gradient = (
        hidden_gradient
        * sigmoid_of_norm
        * (1.0 + normalized_rows * (1.0 - sigmoid_of_norm))
        * channel_norm_gain[:, None]
    )
    average_products, cross_products = packed_total(
        (
            jnp.sum(normed_input_gradient, axis=0),
            jnp.sum(normed_input_gradient * mean_removed, axis=0),
        ),
        "tp",
    )
    conv_output_gradient = inverse_deviation * (
        normed_input_gradient
        - average_products / channel_total
        - mean_removed * (cross_products / channel_total)
    )
    taps_count = conv_taps.shape[0]
    next_rim = from_behind(conv_output_gradient[:, : taps_count - 1], "sp", -1)
    extended = jnp.concatenate([conv_output_gradient, next_rim], axis=1)
    grad_gated = jnp.zeros_like(conv_output_gradient)
    for tap_index in range(taps_count):
        grad_gated = (
            grad_gated
            + conv_taps[tap_index][:, None] * extended[:, tap_index : tap_index + positions]
        )
    gate_sig = jax.nn.sigmoid(conv_gate.astype(jnp.float32))
    grad_value = (grad_gated * gate_sig).astype(jnp.bfloat16)
    grad_gate_in = (
        grad_gated * conv_value.astype(jnp.float32) * gate_sig * (1.0 - gate_sig)
    ).astype(jnp.bfloat16)
    return (grad_gate, grad_up, grad_down, grad_stream, grad_proj, grad_value, grad_gate_in)


def solution(mesh):
    return jax.shard_map(
        body,
        mesh=mesh,
        in_specs=(
            P("sp", None),
            P("sp", None),
            P("sp", None),
            P("sp", None),
            P("sp", None, "tp"),
            P("sp", None, "tp"),
            P("sp", "tp", None),
            P(None, "tp"),
            P("tp", "sp"),
            P("tp", "sp"),
            P(None, "tp"),
            P("tp", "sp"),
            P("tp"),
        ),
        out_specs=(
            P("sp", None, "tp"),
            P("sp", None, "tp"),
            P("sp", "tp", None),
            P("sp", None),
            P("sp", "tp"),
            P("tp", "sp"),
            P("tp", "sp"),
        ),
        check_vma=False,
    )
```

profile of v0, /device:TPU:1, one launch (start us, length us, event | category | flops | bytes accessed | tf_op | source)
XLA Modules:
  0.0 249.6 jit_solution(8566486393356843198)
XLA Ops:
  11.2 1.4 scatter_custom_fusion
  12.7 3.5 %gather_fusion.1 = f32[512]{0:T(512)S(1)} fusion(f32[256]{0:T(256)S(1)} %reshape.203, s32[1024]{0:T(1024)S(1)} %get-tuple-element.78), kind=kCustom, calls=%fused_computation.1 | custom fusion | bytes 6144 | tf_op jit(solution)/shard_map/gather | solution.py:150
  16.3 3.3 %gather_fusion.2 = bf16[512,2048]{1,0:T(8,128)(2,1)} fusion(bf16[128,2048]{1,0:T(8,128)(2,1)S(1)} %copy-done.1, s32[1024]{0:T(1024)S(1)} %get-tuple-element.79), kind=kCustom, calls=%fused_computation.2 | custom fusion | bytes 4196352 | tf_op jit(solution)/shard_map/gather | solution.py:152
  19.6 3.3 %gather_fusion = bf16[512,2048]{1,0:T(8,128)(2,1)} fusion(bf16[128,2048]{1,0:T(8,128)(2,1)S(1)} %copy-done.2, s32[1024]{0:T(1024)S(1)} %get-tuple-element.79), kind=kCustom, calls=%fused_computation | custom fusion | bytes 4196352 | tf_op jit(solution)/shard_map/gather | solution.py:151
  24.0 1.0 dynamic-slice_select_fusion
  25.1 24.9 %all_to_all.32 = bf16[32,32,128]{2,1,0:T(8,128)(2,1)S(1)} all-to-all(bf16[32,32,128]{2,1,0:T(8,128)(2,1)S(1)} %pad_maximum_fusion), channel_id=1, replica_groups=mesh['sp'=32,'tp'=16] {'sp'}, dimensions={0} | all-to-all | bytes 524288 | tf_op jit(solution)/shard_map/all_to_all | solution.py:14
  51.5 9.6 %all-to-all-start.3 = ((f32[16,1,256]{2,1,0:T(1,128)}), f32[16,1,256]{2,1,0:T(1,128)S(1)}, u32[]{:S(2)}, u32[]{:S(2)}) async-start(f32[16,1,256]{2,1,0:T(1,128)} %broadcast_in_dim.59), calls=%async_computation.3 | async-start | bytes 32768 | tf_op jit(solution)/shard_map/all_to_all | solution.py:40
  61.1 39.7 %all-gather.2.cloned.1.call-done = bf16[64,16,2048]{2,1,0:T(8,128)(2,1)} async-done(((bf16[64,16,128]{2,1,0:T(8,128)(2,1)}), bf16[64,16,2048]{2,1,0:T(8,128)(2,1)}) %all-gather.2.cloned.1.call-update) | async-done | bytes 4194320 | tf_op jit(solution)/shard_map/all_gather | solution.py:24
  100.8 2.4 fusion.12
  103.2 2.3 fusion.17
  107.8 1.9 copy.78
  110.4 4.7 %all-to-all-start.1 = ((bf16[16,32,1,16,128]{4,3,1,2,0:T(8,128)(2,1)}), bf16[16,32,1,16,128]{4,3,1,2,0:T(8,128)(2,1)S(1)}, u32[]{:S(2)}, u32[]{:S(2)}) async-start(bf16[16,32,1,16,128]{4,3,1,2,0:T(8,128)(2,1)} %bitcast.245), calls=%async_computation.1 | async-start | bytes 4194304 | tf_op jit(solution)/shard_map/all_to_all | solution.py:34
  115.0 1.3 pad_clamp_fusion
  116.3 1.6 slice_bitcast_fusion.29
  117.9 1.6 slice_bitcast_fusion.30
  119.6 1.3 reduce_sum.101
  120.9 1.3 slice_multiply_fusion.2
  122.2 3.1 %fusion.5 = bf16[1,2048,128]{2,1,0:T(8,128)(2,1)} fusion(bf16[64,16,2048]{2,1,0:T(8,128)(2,1)} %all-gather.2.cloned.1.call-done, bf16[32,1,16,128]{3,2,0,1:T(8,128)(2,1)} %copy-done.7), kind=kOutput, calls=%fused_computation.14 | convolution fusion | flops 268697600 | bytes 4849664 | tf_op jit(solution)/shard_map/secd,secf->edf/dot_general | solution.py:109
  125.4 38.7 %all-to-all-done.1 = bf16[16,32,1,16,128]{4,3,1,2,0:T(8,128)(2,1)S(1)} async-done(((bf16[16,32,1,16,128]{4,3,1,2,0:T(8,128)(2,1)}), bf16[16,32,1,16,128]{4,3,1,2,0:T(8,128)(2,1)S(1)}, u32[]{:S(2)}, u32[]{:S(2)}) %all-to-all-start.1) | async-done | bytes 2097184 | tf_op jit(solution)/shard_map/all_to_all | solution.py:34
  165.1 9.4 %all-to-all-start.2 = ((bf16[32,16,128]{2,1,0:T(8,128)(2,1)}), bf16[32,16,128]{2,1,0:T(8,128)(2,1)S(1)}, u32[]{:S(2)}, u32[]{:S(2)}) async-start(bf16[32,16,128]{2,1,0:T(8,128)(2,1)} %reduce_sum.97), calls=%async_computation.2 | async-start | bytes 262144 | tf_op jit(solution)/shard_map/all_to_all | solution.py:166
  174.5 3.2 %fusion.4 = bf16[1,2048,128]{2,1,0:T(8,128)(2,1)} fusion(bf16[64,16,2048]{2,1,0:T(8,128)(2,1)} %all-gather.2.cloned.1.call-done, bf16[32,1,16,128]{3,2,0,1:T(8,128)(2,1)S(1)} %get-tuple-element.36), kind=kOutput, calls=%fused_computation.13 | convolution fusion | flops 268697600 | bytes 4849664 | tf_op jit(solution)/shard_map/secd,secf->edf/dot_general | solution.py:112
  177.7 6.0 %all-to-all-done.2 = bf16[32,16,128]{2,1,0:T(8,128)(2,1)S(1)} async-done(((bf16[32,16,128]{2,1,0:T(8,128)(2,1)}), bf16[32,16,128]{2,1,0:T(8,128)(2,1)S(1)}, u32[]{:S(2)}, u32[]{:S(2)}) %all-to-all-start.2) | async-done | bytes 131104 | tf_op jit(solution)/shard_map/all_to_all | solution.py:166
  184.9 18.5 %all_gather.7 = bf16[128,2048]{1,0:T(8,128)(2,1)S(1)} all-gather(bf16[128,128]{1,0:T(8,128)(2,1)S(1)} %add_convert_fusion.1), channel_id=1, replica_groups=mesh['sp'=32,'tp'=16] {'tp'}, dimensions={1}, use_global_device_ids=true | all-gather | bytes 557056 | tf_op jit(solution)/shard_map/all_gather | solution.py:169
  204.4 6.0 %all-to-all-start.5 = ((f32[16,1,256]{2,1,0:T(1,128)}), f32[16,1,256]{2,1,0:T(1,128)S(1)}, u32[]{:S(2)}, u32[]{:S(2)}) async-start(f32[16,1,256]{2,1,0:T(1,128)} %broadcast_in_dim.60), calls=%async_computation.5 | async-start | bytes 32768 | tf_op jit(solution)/shard_map/all_to_all | solution.py:40
  212.1 1.4 reshape.267
  213.6 4.2 %all-to-all-done.5 = f32[16,1,256]{2,1,0:T(1,128)S(1)} async-done(((f32[16,1,256]{2,1,0:T(1,128)}), f32[16,1,256]{2,1,0:T(1,128)S(1)}, u32[]{:S(2)}, u32[]{:S(2)}) %all-to-all-start.5) | async-done | bytes 16416 | tf_op jit(solution)/shard_map/all_to_all | solution.py:40
  217.8 3.9 %all-to-all-start.4 = ((f32[32,1,4096]{2,1,0:T(1,128)}), f32[32,1,4096]{2,1,0:T(1,128)S(1)}, u32[]{:S(2)}, u32[]{:S(2)}) async-start(f32[32,1,4096]{2,1,0:T(1,128)} %reshape.267), calls=%async_computation.4 | async-start | bytes 1048576 | tf_op jit(solution)/shard_map/all_to_all | solution.py:57
  221.8 1.3 collective-permute-start
  223.1 3.0 %fusion.3 = bf16[1,128,2048]{2,1,0:T(8,128)(2,1)} fusion(bf16[64,16,2048]{2,1,0:T(8,128)(2,1)} %all-gather.2.cloned.1.call-done, f32[32,16,128]{2,1,0:T(8,128)} %copy-done.5, f32[32,16,128]{2,1,0:T(8,128)S(1)} %fusion.12), kind=kOutput, calls=%fused_computation.12 | convolution fusion | flops 269352960 | bytes 3145728 | tf_op jit(solution)/shard_map/secf,secd->efd/dot_general | solution.py:106
  227.3 1.5 multiply_convert_fusion
  229.4 8.9 %all-to-all-done.4 = f32[32,1,4096]{2,1,0:T(1,128)S(1)} async-done(((f32[32,1,4096]{2,1,0:T(1,128)}), f32[32,1,4096]{2,1,0:T(1,128)S(1)}, u32[]{:S(2)}, u32[]{:S(2)}) %all-to-all-start.4) | async-done | bytes 524320 | tf_op jit(solution)/shard_map/all_to_all | solution.py:57
  238.8 1.9 reduce.6
  (154 shorter events, 18.1 us)
Async XLA Ops:
  7.2 96.1 %copy-start = (bf16[1,2048,128]{2,1,0:T(8,128)(2,1)S(1)}, bf16[1,2048,128]{2,1,0:T(8,128)(2,1)}, u32[]{:S(2)}) copy-start(bf16[1,2048,128]{2,1,0:T(8,128)(2,1)} %param.17) | copy-start | bytes 1572868
  7.2 93.6 %all-gather.2.cloned.1.call-start = ((), (), s32[]{:S(2)}) async-start(), calls=%async_computation.6 | async-start | bytes 4456448 | tf_op jit(solution)/shard_map/all_gather | solution.py:24
  19.6 31.2 %copy-start.6 = (bf16[64,128]{1,0:T(8,128)(2,1)S(1)}, bf16[64,128]{1,0:T(8,128)(2,1)}, u32[]{:S(2)}) copy-start(bf16[64,128]{1,0:T(8,128)(2,1)} %param.24) | copy-start | bytes 49156
  19.6 81.2 %copy-start.4 = (bf16[1,2048,128]{2,1,0:T(8,128)(2,1)S(1)}, bf16[1,2048,128]{2,1,0:T(8,128)(2,1)}, u32[]{:S(2)}) copy-start(bf16[1,2048,128]{2,1,0:T(8,128)(2,1)} %param.18) | copy-start | bytes 1572868
  25.1 80.5 %copy-start.48 = (bf16[1,128,2048]{2,1,0:T(8,128)(2,1)S(1)}, bf16[1,128,2048]{2,1,0:T(8,128)(2,1)}, u32[]{:S(2)}) copy-start(bf16[1,128,2048]{2,1,0:T(8,128)(2,1)} %param.19) | copy-start | bytes 1572868
  51.5 58.3 %all-to-all-start.3 = ((f32[16,1,256]{2,1,0:T(1,128)}), f32[16,1,256]{2,1,0:T(1,128)S(1)}, u32[]{:S(2)}, u32[]{:S(2)}) async-start(f32[16,1,256]{2,1,0:T(1,128)} %broadcast_in_dim.59), calls=%async_computation.3 | async-start | bytes 32768 | tf_op jit(solution)/shard_map/all_to_all | solution.py:40
  110.4 53.7 %all-to-all-start.1 = ((bf16[16,32,1,16,128]{4,3,1,2,0:T(8,128)(2,1)}), bf16[16,32,1,16,128]{4,3,1,2,0:T(8,128)(2,1)S(1)}, u32[]{:S(2)}, u32[]{:S(2)}) async-start(bf16[16,32,1,16,128]{4,3,1,2,0:T(8,128)(2,1)} %bitcast.245), calls=%async_computation.1 | async-start | bytes 4194304 | tf_op jit(solution)/shard_map/all_to_all | solution.py:34
  165.1 18.7 %all-to-all-start.2 = ((bf16[32,16,128]{2,1,0:T(8,128)(2,1)}), bf16[32,16,128]{2,1,0:T(8,128)(2,1)S(1)}, u32[]{:S(2)}, u32[]{:S(2)}) async-start(bf16[32,16,128]{2,1,0:T(8,128)(2,1)} %reduce_sum.97), calls=%async_computation.2 | async-start | bytes 262144 | tf_op jit(solution)/shard_map/all_to_all | solution.py:166
  174.4 29.0 %copy-start.11 = (f32[128]{0:T(128)S(1)}, f32[128]{0:T(128)}, u32[]{:S(2)}) copy-start(f32[128]{0:T(128)} %get-tuple-element.75) | copy-start | bytes 1540
  174.5 29.0 %copy-start.13 = (f32[128]{0:T(128)S(1)}, f32[128]{0:T(128)}, u32[]{:S(2)}) copy-start(f32[128]{0:T(128)} %get-tuple-element.76) | copy-start | bytes 1540
  174.5 29.0 %copy-start.47 = (f32[64]{0:T(128)S(1)}, f32[64]{0:T(128)}, u32[]{:S(2)}) copy-start(f32[64]{0:T(128)} %param.25) | copy-start | bytes 772
  174.5 29.0 %copy-start.49 = (bf16[2048,64]{0,1:T(8,128)(2,1)S(1)}, bf16[2048,64]{0,1:T(8,128)(2,1)}, u32[]{:S(2)}) copy-start(bf16[2048,64]{0,1:T(8,128)(2,1)} %param.20) | copy-start | bytes 786436
  203.4 18.3 %copy-start.12 = (f32[128]{0:T(128)S(1)}, f32[128]{0:T(128)}, u32[]{:S(2)}) copy-start(f32[128]{0:T(128)} %get-tuple-element.75) | copy-start | bytes 1540
  203.4 18.3 %copy-start.14 = (f32[128]{0:T(128)S(1)}, f32[128]{0:T(128)}, u32[]{:S(2)}) copy-start(f32[128]{0:T(128)} %get-tuple-element.76) | copy-start | bytes 1540
  204.4 13.4 %all-to-all-start.5 = ((f32[16,1,256]{2,1,0:T(1,128)}), f32[16,1,256]{2,1,0:T(1,128)S(1)}, u32[]{:S(2)}, u32[]{:S(2)}) async-start(f32[16,1,256]{2,1,0:T(1,128)} %broadcast_in_dim.60), calls=%async_computation.5 | async-start | bytes 32768 | tf_op jit(solution)/shard_map/all_to_all | solution.py:40
  211.2 15.8 %copy-start.8 = (bf16[64,128]{1,0:T(8,128)(2,1)S(1)}, bf16[64,128]{1,0:T(8,128)(2,1)}, u32[]{:S(2)}) copy-start(bf16[64,128]{1,0:T(8,128)(2,1)} %param.22) | copy-start | bytes 49156
  211.2 15.8 %copy-start.10 = (bf16[64,128]{1,0:T(8,128)(2,1)S(1)}, bf16[64,128]{1,0:T(8,128)(2,1)}, u32[]{:S(2)}) copy-start(bf16[64,128]{1,0:T(8,128)(2,1)} %param.21) | copy-start | bytes 49156
  211.2 15.8 %copy-start.16 = (f32[64]{0:T(128)S(1)}, f32[64]{0:T(128)}, u32[]{:S(2)}) copy-start(f32[64]{0:T(128)} %get-tuple-element.59) | copy-start | bytes 772
  211.2 15.8 %copy-start.17 = (f32[64]{0:T(128)S(1)}, f32[64]{0:T(128)}, u32[]{:S(2)}) copy-start(f32[64]{0:T(128)} %get-tuple-element.60) | copy-start | bytes 772
  211.2 15.8 %copy-start.18 = (f32[64]{0:T(128)S(1)}, f32[64]{0:T(128)}, u32[]{:S(2)}) copy-start(f32[64]{0:T(128)} %get-tuple-element.61) | copy-start | bytes 772
  211.2 15.8 %copy-start.19 = (f32[64]{0:T(128)S(1)}, f32[64]{0:T(128)}, u32[]{:S(2)}) copy-start(f32[64]{0:T(128)} %get-tuple-element.62) | copy-start | bytes 772
  211.2 15.8 %copy-start.20 = (f32[64]{0:T(128)S(1)}, f32[64]{0:T(128)}, u32[]{:S(2)}) copy-start(f32[64]{0:T(128)} %get-tuple-element.63) | copy-start | bytes 772
  211.2 15.8 %copy-start.21 = (f32[64]{0:T(128)S(1)}, f32[64]{0:T(128)}, u32[]{:S(2)}) copy-start(f32[64]{0:T(128)} %get-tuple-element.64) | copy-start | bytes 772
  211.3 15.8 %copy-start.22 = (f32[64]{0:T(128)S(1)}, f32[64]{0:T(128)}, u32[]{:S(2)}) copy-start(f32[64]{0:T(128)} %get-tuple-element.65) | copy-start | bytes 772
  211.3 15.8 %copy-start.23 = (f32[64]{0:T(128)S(1)}, f32[64]{0:T(128)}, u32[]{:S(2)}) copy-start(f32[64]{0:T(128)} %get-tuple-element.66) | copy-start | bytes 772
  211.3 15.8 %copy-start.24 = (f32[64]{0:T(128)S(1)}, f32[64]{0:T(128)}, u32[]{:S(2)}) copy-start(f32[64]{0:T(128)} %get-tuple-element.67) | copy-start | bytes 772
  211.3 15.8 %copy-start.25 = (f32[64]{0:T(128)S(1)}, f32[64]{0:T(128)}, u32[]{:S(2)}) copy-start(f32[64]{0:T(128)} %get-tuple-element.68) | copy-start | bytes 772
  211.9 15.1 %copy-start.26 = (f32[64]{0:T(128)S(1)}, f32[64]{0:T(128)}, u32[]{:S(2)}) copy-start(f32[64]{0:T(128)} %get-tuple-element.69) | copy-start | bytes 772
  211.9 15.1 %copy-start.27 = (f32[64]{0:T(128)S(1)}, f32[64]{0:T(128)}, u32[]{:S(2)}) copy-start(f32[64]{0:T(128)} %get-tuple-element.70) | copy-start | bytes 772
  211.9 15.1 %copy-start.28 = (f32[64]{0:T(128)S(1)}, f32[64]{0:T(128)}, u32[]{:S(2)}) copy-start(f32[64]{0:T(128)} %get-tuple-element.40) | copy-start | bytes 772
  217.8 20.5 %all-to-all-start.4 = ((f32[32,1,4096]{2,1,0:T(1,128)}), f32[32,1,4096]{2,1,0:T(1,128)S(1)}, u32[]{:S(2)}, u32[]{:S(2)}) async-start(f32[32,1,4096]{2,1,0:T(1,128)} %reshape.267), calls=%async_computation.4 | async-start | bytes 1048576 | tf_op jit(solution)/shard_map/all_to_all | solution.py:57
  221.8 5.2 %collective-permute-start = (f32[64,30]{1,0:T(8,128)S(1)}, f32[64,30]{1,0:T(8,128)S(1)}, u32[]{:S(2)}, u32[]{:S(2)}) collective-permute-start(f32[64,30]{1,0:T(8,128)S(1)} %bitcast.253), channel_id=1, source_target_pairs={{16,0},{32,16},{48,32},{64,48},{80,64},{96,80},{112,96},{128,112},... | collective-permute-start | bytes 23048 | tf_op jit(solution)/shard_map/ppermute | solution.py:64
  (25 other events, 294.9 us)
Sparse Core Ops, SparseCore 0:
  50.9 49.7 all-gather.1
where the time goes:
time: 250 us
  waiting for transfers between devices  98.5 us (39%)
  blocking collectives  43.5 us (17%)
  starting transfers between devices  34.9 us (14%)
  local copies, waits for them, and re-layouts  27.2 us (11%)
  matrix products  16.9 us (7%)
  between operations  15 us (6%)
  other arithmetic  13.7 us (5%)
    all_gather x1, waiting for transfers between devices, sent_together_2(): lax.all_gather(both, axis, axis=dim, tiled=True)  39.7 us
    all_to_all x1, waiting for transfers between devices, summed_on_arrival(): lax.all_to_all(tiles, axis, split_axis=0, concat_axis=0, tiled=True)  38.7 us
    all_to_all x1, blocking collectives, sent_together(): lax.all_to_all(both, axis, split_axis=split_dim, concat_axis=concat_dim,...  24.9 us
    all_gather x1, blocking collectives, body(): grad_stream = lax.all_gather(stream_part, 'tp', axis=1, tiled=True)  18.5 us
    all_to_all x2, starting transfers between devices, copy_for_each(): return lax.all_to_all(copies, axis, split_axis=0, concat_axis=0, tiled=True)  15.6 us
    all_to_all x1, starting transfers between devices, body(): lax.all_to_all(returned, 'sp', split_axis=0, concat_axis=0, tiled=True)  9.38 us
    all_to_all x1, waiting for transfers between devices, summed_on_arrival_2(): lax.all_to_all(cut_along(array, dim, devices), axis, 0, 0, tiled=True)  8.92 us
    all_to_all x1, waiting for transfers between devices, body(): lax.all_to_all(returned, 'sp', split_axis=0, concat_axis=0, tiled=True)  6.04 us
  transfers between devices with their start and end apart: 7, of which 6 were waited for; matrix products, arithmetic and copies ran while one was open for 12% of the time, Pallas kernels for 0%

commit v1 on v0

--- a/solution.py
+++ b/solution.py
@@ -166,7 +166,8 @@
     returned = lax.all_to_all(returned, "sp", split_axis=0, concat_axis=0, tiled=True)
     cot_cols = lax.dynamic_slice_in_dim(out_cot, slice_start, slice_width, 1)
     stream_part = combine_routes(returned, slot_of, cot_cols, token_rows, top_count)
-    grad_stream = lax.all_gather(stream_part, "tp", axis=1, tiled=True)
+    sent = jnp.stack([stream_part] * lax.axis_size("tp"))
+    grad_stream = jnp.concatenate(lax.all_to_all(sent, "tp", 0, 0), axis=1)
     channel_total = conv_result.shape[0] * tp_count
     positions = conv_result.shape[1]
     conv_float = conv_result.astype(jnp.float32)

time: 250 us -> 264 us (1.056)
  waiting for transfers between devices: 98.5 us -> 136 us
  blocking collectives: 43.5 us -> 24.9 us
    all_gather x1 -> x0, blocking collectives: 18.5 us -> none  [body(): grad_stream = lax.all_gather(stream_part, 'tp', axis=1, tiled=True)]
    all_to_all x0 -> x1, waiting for transfers between devices: none -> 12.4 us  [body(): grad_stream = jnp.concatenate(lax.all_to_all(sent, 'tp', 0, 0), axis=1)]
    all_gather x1, waiting for transfers between devices: 39.7 us -> 50.3 us  [sent_together_2(): lax.all_gather(both, axis, axis=dim, tiled=True)]
    all_to_all x1, waiting for transfers between devices: 38.7 us -> 46.9 us  [summed_on_arrival(): lax.all_to_all(tiles, axis, split_axis=0, concat_axis=0, tiled=True)]
    all_to_all x2, starting transfers between devices: 15.6 us -> 8.23 us  [copy_for_each(): return lax.all_to_all(copies, axis, split_axis=0, concat_axis=0, tiled=True)]
    all_to_all x0 -> x1, starting transfers between devices: none -> 5.45 us  [body(): grad_stream = jnp.concatenate(lax.all_to_all(sent, 'tp', 0, 0), axis=1)]
    all_to_all x2, waiting for transfers between devices: 4.23 us -> 9.65 us  [copy_for_each(): return lax.all_to_all(copies, axis, split_axis=0, concat_axis=0, tiled=True)]
    unnamed x106 -> x99, local copies, waits for them, and re-layouts: 5.75 us -> 4.68 us
  transfers between devices with their start and end apart: 7 -> 8, of which waited for: 6 -> 7; matrix products, arithmetic and copies ran while one was open for 12% -> 7% of each run, Pallas kernels for 0% -> 0%
where the time goes in v1:
time: 264 us; the launch traced here: 263 us
  waiting for transfers between devices  136 us (52%)
  starting transfers between devices  32.4 us (12%)
  local copies, waits for them, and re-layouts  26.8 us (10%)
  blocking collectives  24.9 us (9%)
  matrix products  15.4 us (6%)
  between operations  14.9 us (6%)
  other arithmetic  12.4 us (5%)
    all_gather x1, waiting for transfers between devices, sent_together_2(): lax.all_gather(both, axis, axis=dim, tiled=True)  50.3 us
    all_to_all x1, waiting for transfers between devices, summed_on_arrival(): lax.all_to_all(tiles, axis, split_axis=0, concat_axis=0, tiled=True)  46.9 us
    all_to_all x1, blocking collectives, sent_together(): lax.all_to_all(both, axis, split_axis=split_dim, concat_axis=concat_dim,...  24.9 us
    all_to_all x1, waiting for transfers between devices, body(): grad_stream = jnp.concatenate(lax.all_to_all(sent, 'tp', 0, 0), axis=1)  12.4 us
    all_to_all x1, starting transfers between devices, body(): lax.all_to_all(returned, 'sp', split_axis=0, concat_axis=0, tiled=True)  9.69 us
    all_to_all x2, waiting for transfers between devices, copy_for_each(): return lax.all_to_all(copies, axis, split_axis=0, concat_axis=0, tiled=True)  9.65 us
    all_to_all x1, waiting for transfers between devices, summed_on_arrival_2(): lax.all_to_all(cut_along(array, dim, devices), axis, 0, 0, tiled=True)  8.85 us
    all_to_all x2, starting transfers between devices, copy_for_each(): return lax.all_to_all(copies, axis, split_axis=0, concat_axis=0, tiled=True)  8.23 us
  transfers between devices with their start and end apart: 8, of which 7 were waited for; matrix products, arithmetic and copies ran while one was open for 7% of the time, Pallas kernels for 0%

profile of v1, /device:TPU:1, one launch (start us, length us, event | category | flops | bytes accessed | tf_op | source)
XLA Modules:
  0.0 262.7 jit_solution(16035389105693923300)
XLA Ops:
  11.2 1.4 scatter_custom_fusion
  12.7 3.5 %gather_fusion.1 = f32[512]{0:T(512)S(1)} fusion(f32[256]{0:T(256)S(1)} %reshape.210, s32[1024]{0:T(1024)S(1)} %get-tuple-element.78), kind=kCustom, calls=%fused_computation.1 | custom fusion | bytes 6144 | tf_op jit(solution)/shard_map/gather | solution.py:150
  16.3 3.3 %gather_fusion.2 = bf16[512,2048]{1,0:T(8,128)(2,1)} fusion(bf16[128,2048]{1,0:T(8,128)(2,1)S(1)} %copy-done.1, s32[1024]{0:T(1024)S(1)} %get-tuple-element.79), kind=kCustom, calls=%fused_computation.2 | custom fusion | bytes 4196352 | tf_op jit(solution)/shard_map/gather | solution.py:152
  19.6 3.3 %gather_fusion = bf16[512,2048]{1,0:T(8,128)(2,1)} fusion(bf16[128,2048]{1,0:T(8,128)(2,1)S(1)} %copy-done.2, s32[1024]{0:T(1024)S(1)} %get-tuple-element.79), kind=kCustom, calls=%fused_computation | custom fusion | bytes 4196352 | tf_op jit(solution)/shard_map/gather | solution.py:151
  24.0 1.0 dynamic-slice_select_fusion
  25.1 24.9 %all_to_all.37 = bf16[32,32,128]{2,1,0:T(8,128)(2,1)S(1)} all-to-all(bf16[32,32,128]{2,1,0:T(8,128)(2,1)S(1)} %pad_maximum_fusion), channel_id=1, replica_groups=mesh['sp'=32,'tp'=16] {'sp'}, dimensions={0} | all-to-all | bytes 524288 | tf_op jit(solution)/shard_map/all_to_all | solution.py:14
  50.8 50.3 %all-gather.2.cloned.1.call-done = bf16[64,16,2048]{2,1,0:T(8,128)(2,1)} async-done(((bf16[64,16,128]{2,1,0:T(8,128)(2,1)}), bf16[64,16,2048]{2,1,0:T(8,128)(2,1)}) %all-gather.2.cloned.1.call-update) | async-done | bytes 4194320 | tf_op jit(solution)/shard_map/all_gather | solution.py:24
  101.1 2.4 fusion.12
  103.6 2.3 fusion.17
  108.2 1.9 copy.82
  110.1 3.8 %all-to-all-start.1 = ((bf16[16,32,1,16,128]{4,3,1,2,0:T(8,128)(2,1)}), bf16[16,32,1,16,128]{4,3,1,2,0:T(8,128)(2,1)S(1)}, u32[]{:S(2)}, u32[]{:S(2)}) async-start(bf16[16,32,1,16,128]{4,3,1,2,0:T(8,128)(2,1)} %bitcast.254), calls=%async_computation.1 | async-start | bytes 4194304 | tf_op jit(solution)/shard_map/all_to_all | solution.py:34
  114.5 1.6 slice_bitcast_fusion.30
  116.1 46.9 %all-to-all-done.1 = bf16[16,32,1,16,128]{4,3,1,2,0:T(8,128)(2,1)S(1)} async-done(((bf16[16,32,1,16,128]{4,3,1,2,0:T(8,128)(2,1)}), bf16[16,32,1,16,128]{4,3,1,2,0:T(8,128)(2,1)S(1)}, u32[]{:S(2)}, u32[]{:S(2)}) %all-to-all-start.1) | async-done | bytes 2097184 | tf_op jit(solution)/shard_map/all_to_all | solution.py:34
  163.0 1.3 broadcast_in_dim.59
  164.3 4.8 %all-to-all-start.4 = ((f32[16,1,256]{2,1,0:T(1,128)}), f32[16,1,256]{2,1,0:T(1,128)}, u32[]{:S(2)}, u32[]{:S(2)}) async-start(f32[16,1,256]{2,1,0:T(1,128)} %broadcast_in_dim.59), calls=%async_computation.4 | async-start | bytes 32768 | tf_op jit(solution)/shard_map/all_to_all | solution.py:40
  169.1 1.6 slice_bitcast_fusion.29
  171.7 4.9 %all-to-all-done.4 = f32[16,1,256]{2,1,0:T(1,128)} async-done(((f32[16,1,256]{2,1,0:T(1,128)}), f32[16,1,256]{2,1,0:T(1,128)}, u32[]{:S(2)}, u32[]{:S(2)}) %all-to-all-start.4) | async-done | bytes 16416 | tf_op jit(solution)/shard_map/all_to_all | solution.py:40
  176.6 9.7 %all-to-all-start.2 = ((bf16[32,16,128]{2,1,0:T(8,128)(2,1)}), bf16[32,16,128]{2,1,0:T(8,128)(2,1)S(1)}, u32[]{:S(2)}, u32[]{:S(2)}) async-start(bf16[32,16,128]{2,1,0:T(8,128)(2,1)} %reduce_sum.97), calls=%async_computation.2 | async-start | bytes 262144 | tf_op jit(solution)/shard_map/all_to_all | solution.py:166
  187.7 7.9 %all-to-all-done.2 = bf16[32,16,128]{2,1,0:T(8,128)(2,1)S(1)} async-done(((bf16[32,16,128]{2,1,0:T(8,128)(2,1)}), bf16[32,16,128]{2,1,0:T(8,128)(2,1)S(1)}, u32[]{:S(2)}, u32[]{:S(2)}) %all-to-all-start.2) | async-done | bytes 131104 | tf_op jit(solution)/shard_map/all_to_all | solution.py:166
  197.6 5.5 %all-to-all-start.3 = ((bf16[16,128,128]{2,1,0:T(8,128)(2,1)}), bf16[16,128,128]{2,1,0:T(8,128)(2,1)S(1)}, u32[]{:S(2)}, u32[]{:S(2)}) async-start(bf16[16,128,128]{2,1,0:T(8,128)(2,1)} %stack.2), calls=%async_computation.3 | async-start | bytes 1048576 | tf_op jit(solution)/shard_map/all_to_all | solution.py:170
  203.0 3.3 %fusion.5 = bf16[1,2048,128]{2,1,0:T(8,128)(2,1)} fusion(bf16[64,16,2048]{2,1,0:T(8,128)(2,1)} %all-gather.2.cloned.1.call-done, bf16[32,1,16,128]{3,2,0,1:T(8,128)(2,1)} %copy-done.10), kind=kOutput, calls=%fused_computation.14 | convolution fusion | flops 268697600 | bytes 4849664 | tf_op jit(solution)/shard_map/secd,secf->edf/dot_general | solution.py:109
  206.3 1.6 fusion.4
  207.9 12.4 %all-to-all-done.3 = bf16[16,128,128]{2,1,0:T(8,128)(2,1)S(1)} async-done(((bf16[16,128,128]{2,1,0:T(8,128)(2,1)}), bf16[16,128,128]{2,1,0:T(8,128)(2,1)S(1)}, u32[]{:S(2)}, u32[]{:S(2)}) %all-to-all-start.3) | async-done | bytes 524320 | tf_op jit(solution)/shard_map/all_to_all | solution.py:170
  221.4 3.4 %all-to-all-start.6 = ((f32[16,1,256]{2,1,0:T(1,128)}), f32[16,1,256]{2,1,0:T(1,128)S(1)}, u32[]{:S(2)}, u32[]{:S(2)}) async-start(f32[16,1,256]{2,1,0:T(1,128)} %broadcast_in_dim.60), calls=%async_computation.6 | async-start | bytes 32768 | tf_op jit(solution)/shard_map/all_to_all | solution.py:40
  225.6 1.5 reshape.276
  227.0 4.8 %all-to-all-done.6 = f32[16,1,256]{2,1,0:T(1,128)S(1)} async-done(((f32[16,1,256]{2,1,0:T(1,128)}), f32[16,1,256]{2,1,0:T(1,128)S(1)}, u32[]{:S(2)}, u32[]{:S(2)}) %all-to-all-start.6) | async-done | bytes 16416 | tf_op jit(solution)/shard_map/all_to_all | solution.py:40
  231.8 3.9 %all-to-all-start.5 = ((f32[32,1,4096]{2,1,0:T(1,128)}), f32[32,1,4096]{2,1,0:T(1,128)S(1)}, u32[]{:S(2)}, u32[]{:S(2)}) async-start(f32[32,1,4096]{2,1,0:T(1,128)} %reshape.276), calls=%async_computation.5 | async-start | bytes 1048576 | tf_op jit(solution)/shard_map/all_to_all | solution.py:57
  235.7 1.3 collective-permute-start
  237.1 2.9 %fusion.3 = bf16[1,128,2048]{2,1,0:T(8,128)(2,1)} fusion(bf16[64,16,2048]{2,1,0:T(8,128)(2,1)} %all-gather.2.cloned.1.call-done, f32[32,16,128]{2,1,0:T(8,128)S(1)} %copy-done.9, f32[32,16,128]{2,1,0:T(8,128)S(1)} %fusion.12), kind=kOutput, calls=%fused_computation.12 | convolution fusion | flops 269352960 | bytes 3145728 | tf_op jit(solution)/shard_map/secf,secd->efd/dot_general | solution.py:106
  241.3 1.5 multiply_convert_fusion
  243.5 8.9 %all-to-all-done.5 = f32[32,1,4096]{2,1,0:T(1,128)S(1)} async-done(((f32[32,1,4096]{2,1,0:T(1,128)}), f32[32,1,4096]{2,1,0:T(1,128)S(1)}, u32[]{:S(2)}, u32[]{:S(2)}) %all-to-all-start.5) | async-done | bytes 524320 | tf_op jit(solution)/shard_map/all_to_all | solution.py:57
  252.8 1.9 reduce.6
  (148 shorter events, 18.2 us)
Async XLA Ops:
  7.2 96.4 %copy-start = (bf16[1,2048,128]{2,1,0:T(8,128)(2,1)S(1)}, bf16[1,2048,128]{2,1,0:T(8,128)(2,1)}, u32[]{:S(2)}) copy-start(bf16[1,2048,128]{2,1,0:T(8,128)(2,1)} %param.17) | copy-start | bytes 1572868
  7.2 93.9 %all-gather.2.cloned.1.call-start = ((), (), s32[]{:S(2)}) async-start(), calls=%async_computation.7 | async-start | bytes 4456448 | tf_op jit(solution)/shard_map/all_gather | solution.py:24
  19.6 81.5 %copy-start.5 = (bf16[1,2048,128]{2,1,0:T(8,128)(2,1)S(1)}, bf16[1,2048,128]{2,1,0:T(8,128)(2,1)}, u32[]{:S(2)}) copy-start(bf16[1,2048,128]{2,1,0:T(8,128)(2,1)} %param.18) | copy-start | bytes 1572868
  25.0 80.8 %copy-start.46 = (bf16[1,128,2048]{2,1,0:T(8,128)(2,1)S(1)}, bf16[1,128,2048]{2,1,0:T(8,128)(2,1)}, u32[]{:S(2)}) copy-start(bf16[1,128,2048]{2,1,0:T(8,128)(2,1)} %param.19) | copy-start | bytes 1572868
  110.1 52.9 %all-to-all-start.1 = ((bf16[16,32,1,16,128]{4,3,1,2,0:T(8,128)(2,1)}), bf16[16,32,1,16,128]{4,3,1,2,0:T(8,128)(2,1)S(1)}, u32[]{:S(2)}, u32[]{:S(2)}) async-start(bf16[16,32,1,16,128]{4,3,1,2,0:T(8,128)(2,1)} %bitcast.254), calls=%async_computation.1 | async-start | bytes 4194304 | tf_op jit(solution)/shard_map/all_to_all | solution.py:34
  164.3 12.3 %all-to-all-start.4 = ((f32[16,1,256]{2,1,0:T(1,128)}), f32[16,1,256]{2,1,0:T(1,128)}, u32[]{:S(2)}, u32[]{:S(2)}) async-start(f32[16,1,256]{2,1,0:T(1,128)} %broadcast_in_dim.59), calls=%async_computation.4 | async-start | bytes 32768 | tf_op jit(solution)/shard_map/all_to_all | solution.py:40
  176.6 19.0 %all-to-all-start.2 = ((bf16[32,16,128]{2,1,0:T(8,128)(2,1)}), bf16[32,16,128]{2,1,0:T(8,128)(2,1)S(1)}, u32[]{:S(2)}, u32[]{:S(2)}) async-start(bf16[32,16,128]{2,1,0:T(8,128)(2,1)} %reduce_sum.97), calls=%async_computation.2 | async-start | bytes 262144 | tf_op jit(solution)/shard_map/all_to_all | solution.py:166
  197.6 22.7 %all-to-all-start.3 = ((bf16[16,128,128]{2,1,0:T(8,128)(2,1)}), bf16[16,128,128]{2,1,0:T(8,128)(2,1)S(1)}, u32[]{:S(2)}, u32[]{:S(2)}) async-start(bf16[16,128,128]{2,1,0:T(8,128)(2,1)} %stack.2), calls=%async_computation.3 | async-start | bytes 1048576 | tf_op jit(solution)/shard_map/all_to_all | solution.py:170
  207.9 29.1 %copy-start.9 = (f32[32,16,128]{2,1,0:T(8,128)S(1)}, f32[32,16,128]{2,1,0:T(8,128)}, u32[]{:S(2)}) copy-start(f32[32,16,128]{2,1,0:T(8,128)} %copy-done.8) | copy-start | bytes 786436
  221.4 10.3 %all-to-all-start.6 = ((f32[16,1,256]{2,1,0:T(1,128)}), f32[16,1,256]{2,1,0:T(1,128)S(1)}, u32[]{:S(2)}, u32[]{:S(2)}) async-start(f32[16,1,256]{2,1,0:T(1,128)} %broadcast_in_dim.60), calls=%async_computation.6 | async-start | bytes 32768 | tf_op jit(solution)/shard_map/all_to_all | solution.py:40
  224.8 16.2 %copy-start.11 = (bf16[64,128]{1,0:T(8,128)(2,1)S(1)}, bf16[64,128]{1,0:T(8,128)(2,1)}, u32[]{:S(2)}) copy-start(bf16[64,128]{1,0:T(8,128)(2,1)} %param.22) | copy-start | bytes 49156
  224.9 16.1 %copy-start.12 = (bf16[64,128]{1,0:T(8,128)(2,1)S(1)}, bf16[64,128]{1,0:T(8,128)(2,1)}, u32[]{:S(2)}) copy-start(bf16[64,128]{1,0:T(8,128)(2,1)} %param.21) | copy-start | bytes 49156
  224.9 16.1 %copy-start.15 = (f32[64]{0:T(128)S(1)}, f32[64]{0:T(128)}, u32[]{:S(2)}) copy-start(f32[64]{0:T(128)} %get-tuple-element.40) | copy-start | bytes 772
  224.9 16.1 %copy-start.16 = (f32[64]{0:T(128)S(1)}, f32[64]{0:T(128)}, u32[]{:S(2)}) copy-start(f32[64]{0:T(128)} %get-tuple-element.41) | copy-start | bytes 772
  224.9 16.1 %copy-start.17 = (f32[64]{0:T(128)S(1)}, f32[64]{0:T(128)}, u32[]{:S(2)}) copy-start(f32[64]{0:T(128)} %get-tuple-element.42) | copy-start | bytes 772
  224.9 16.1 %copy-start.18 = (f32[64]{0:T(128)S(1)}, f32[64]{0:T(128)}, u32[]{:S(2)}) copy-start(f32[64]{0:T(128)} %get-tuple-element.43) | copy-start | bytes 772
  224.9 16.1 %copy-start.19 = (f32[64]{0:T(128)S(1)}, f32[64]{0:T(128)}, u32[]{:S(2)}) copy-start(f32[64]{0:T(128)} %get-tuple-element.44) | copy-start | bytes 772
  224.9 16.1 %copy-start.20 = (f32[64]{0:T(128)S(1)}, f32[64]{0:T(128)}, u32[]{:S(2)}) copy-start(f32[64]{0:T(128)} %get-tuple-element.45) | copy-start | bytes 772
  224.9 16.1 %copy-start.21 = (f32[64]{0:T(128)S(1)}, f32[64]{0:T(128)}, u32[]{:S(2)}) copy-start(f32[64]{0:T(128)} %get-tuple-element.46) | copy-start | bytes 772
  224.9 16.1 %copy-start.22 = (f32[64]{0:T(128)S(1)}, f32[64]{0:T(128)}, u32[]{:S(2)}) copy-start(f32[64]{0:T(128)} %get-tuple-element.47) | copy-start | bytes 772
  225.0 16.1 %copy-start.23 = (f32[64]{0:T(128)S(1)}, f32[64]{0:T(128)}, u32[]{:S(2)}) copy-start(f32[64]{0:T(128)} %get-tuple-element.48) | copy-start | bytes 772
  225.0 16.1 %copy-start.24 = (f32[64]{0:T(128)S(1)}, f32[64]{0:T(128)}, u32[]{:S(2)}) copy-start(f32[64]{0:T(128)} %get-tuple-element.49) | copy-start | bytes 772
  225.0 16.1 %copy-start.25 = (f32[64]{0:T(128)S(1)}, f32[64]{0:T(128)}, u32[]{:S(2)}) copy-start(f32[64]{0:T(128)} %get-tuple-element.50) | copy-start | bytes 772
  225.0 16.1 %copy-start.26 = (f32[64]{0:T(128)S(1)}, f32[64]{0:T(128)}, u32[]{:S(2)}) copy-start(f32[64]{0:T(128)} %get-tuple-element.51) | copy-start | bytes 772
  225.0 16.1 %copy-start.27 = (f32[64]{0:T(128)S(1)}, f32[64]{0:T(128)}, u32[]{:S(2)}) copy-start(f32[64]{0:T(128)} %get-tuple-element.52) | copy-start | bytes 772
  225.0 16.1 %copy-start.28 = (f32[64]{0:T(128)S(1)}, f32[64]{0:T(128)}, u32[]{:S(2)}) copy-start(f32[64]{0:T(128)} %get-tuple-element.53) | copy-start | bytes 772
  225.0 16.1 %copy-start.29 = (f32[64]{0:T(128)S(1)}, f32[64]{0:T(128)}, u32[]{:S(2)}) copy-start(f32[64]{0:T(128)} %get-tuple-element.54) | copy-start | bytes 772
  225.0 16.1 %copy-start.30 = (f32[64]{0:T(128)S(1)}, f32[64]{0:T(128)}, u32[]{:S(2)}) copy-start(f32[64]{0:T(128)} %get-tuple-element.55) | copy-start | bytes 772
  225.0 16.1 %copy-start.31 = (f32[64]{0:T(128)S(1)}, f32[64]{0:T(128)}, u32[]{:S(2)}) copy-start(f32[64]{0:T(128)} %get-tuple-element.56) | copy-start | bytes 772
  225.0 16.1 %copy-start.32 = (f32[64]{0:T(128)S(1)}, f32[64]{0:T(128)}, u32[]{:S(2)}) copy-start(f32[64]{0:T(128)} %get-tuple-element.57) | copy-start | bytes 772
  231.8 20.5 %all-to-all-start.5 = ((f32[32,1,4096]{2,1,0:T(1,128)}), f32[32,1,4096]{2,1,0:T(1,128)S(1)}, u32[]{:S(2)}, u32[]{:S(2)}) async-start(f32[32,1,4096]{2,1,0:T(1,128)} %reshape.276), calls=%async_computation.5 | async-start | bytes 1048576 | tf_op jit(solution)/shard_map/all_to_all | solution.py:57
  235.7 5.3 %collective-permute-start = (f32[64,30]{1,0:T(8,128)S(1)}, f32[64,30]{1,0:T(8,128)S(1)}, u32[]{:S(2)}, u32[]{:S(2)}) collective-permute-start(f32[64,30]{1,0:T(8,128)S(1)} %bitcast.259), channel_id=1, source_target_pairs={{16,0},{32,16},{48,32},{64,48},{80,64},{96,80},{112,96},{128,112},... | collective-permute-start | bytes 23048 | tf_op jit(solution)/shard_map/ppermute | solution.py:64
  (23 other events, 268.9 us)
Sparse Core Ops, SparseCore 0:
  50.9 50.1 all-gather.1
